TPU v7x, 256 devices: a whole 4x4x8 slice. The times are simulated.
256 devices in a mesh: sp: 16 (over y, x), dp: 16 (over z, core).
Axes of the slice: x: 4, y: 4, z: 8, core: 2. Of those that a mesh axis runs over, the one named last changes fastest.
Arguments:
- tokens: bfloat16 [16, 6144, 2048], P('dp', 'sp'), may hold values from -6 to 6
- value_act: bfloat16 [16, 6144, 1024], P('dp', 'sp'), may hold values from -6 to 6
- gate_act: bfloat16 [16, 6144, 1024], P('dp', 'sp'), may hold values from -6 to 6
- cotangent: bfloat16 [16, 6144, 1024], P('dp', 'sp'), may hold values from -6 to 6
- value_weight: bfloat16 [2048, 1024], P('dp'), may hold values from -0.1875 to 0.1875
- gate_weight: bfloat16 [2048, 1024], P('dp'), may hold values from -0.1875 to 0.1875
- norm_gain: float32 [1024], replicated, may hold values from 0.1 to 1.9
- norm_bias: float32 [1024], replicated, may hold values from -3 to 3
- mix_weight: bfloat16 [16, 128, 128], replicated, may hold values from -0.5 to 0.5
- mix_bias: float32 [16, 128], replicated, may hold values from 0.1 to 1.9
Outputs:
- tokens_grad: bfloat16 [16, 6144, 2048], P('dp', 'sp')
- value_weight_grad: float32 [2048, 1024], P('dp')
- gate_weight_grad: float32 [2048, 1024], P('dp')
- mix_weight_grad: float32 [16, 128, 128], replicated
- mix_bias_grad: float32 [16, 128], replicated
- norm_gain_grad: float32 [1024], replicated
- norm_bias_grad: float32 [1024], replicated
All inputs are finite; a program needn't handle non-finite values.
Results may differ from a plain program's by a relative error of at most 0.0054.
Values may be sent and summed in bfloat16 or wider, within the bound.
A program may use at most 128 MiB of HBM per device.

v0:
```python
import jax
import jax.numpy as jnp
from jax import lax
from jax.sharding import PartitionSpec as P

EPSILON = 1e-06


def gelu_slope(values):
    cdf_part = 0.5 * (1.0 + lax.erf(values * 0.7071067811865476))
    pdf_part = jnp.exp(-0.5 * values * values) * 0.3989422804014327
    return cdf_part + values * pdf_part


def mixer_backward(value_act, gate_act, cotangent, norm_gain, norm_bias, mix_weight, mix_bias):
    seq_len, channels = value_act.shape
    groups, block_len = (mix_weight.shape[0], mix_weight.shape[1])
    group_dim = channels // groups
    blocks = seq_len // block_len
    value_float = value_act.astype(jnp.float32)
    gate_float = gate_act.astype(jnp.float32)
    activated = jax.nn.gelu(value_float, approximate=False)
    gate_gelu = jax.nn.gelu(gate_float, approximate=False)
    centred = gate_gelu - jnp.mean(gate_gelu, axis=-1, keepdims=True)
    inv_std = lax.rsqrt(jnp.mean(centred * centred, axis=-1, keepdims=True) + EPSILON)
    normed = centred * inv_std
    spread_in = (normed * norm_gain + norm_bias).astype(jnp.bfloat16)
    spread_in = spread_in.reshape(blocks, block_len, groups, group_dim)
    causal = jnp.tril(jnp.ones((block_len, block_len), dtype=bool))
    masked_weight = jnp.where(causal[None], mix_weight, jnp.zeros_like(mix_weight))
    spatial = jnp.einsum(
        "gts,bsgd->btgd", masked_weight, spread_in, preferred_element_type=jnp.float32
    )
    spatial = (spatial + mix_bias.T[None, :, :, None]).reshape(seq_len, channels)
    grad_out = cotangent.astype(jnp.float32)
    grad_act = grad_out * spatial
    grad_spatial = grad_out * activated
    grad_split = grad_spatial.reshape(blocks, block_len, groups, group_dim)
    bias_grad = jnp.sum(grad_split, axis=(0, 3)).T
    spatial_low = grad_split.astype(jnp.bfloat16)
    weight_grad = jnp.einsum(
        "btgd,bsgd->gts", spatial_low, spread_in, preferred_element_type=jnp.float32
    )
    weight_grad = jnp.where(causal[None], weight_grad, jnp.zeros_like(weight_grad))
    grad_norm = jnp.einsum(
        "gts,btgd->bsgd", masked_weight, spatial_low, preferred_element_type=jnp.float32
    )
    grad_norm = grad_norm.reshape(seq_len, channels)
    gain_grad = jnp.sum(grad_norm * normed, axis=0)
    shift_grad = jnp.sum(grad_norm, axis=0)
    grad_hat = grad_norm * norm_gain
    grad_gate = inv_std * (
        grad_hat
        - jnp.mean(grad_hat, axis=-1, keepdims=True)
        - normed * jnp.mean(grad_hat * normed, axis=-1, keepdims=True)
    )
    value_grad = (grad_act * gelu_slope(value_float)).astype(jnp.bfloat16)
    gate_grad = (grad_gate * gelu_slope(gate_float)).astype(jnp.bfloat16)
    return (value_grad, gate_grad, (weight_grad, bias_grad, gain_grad, shift_grad))


def shards(
    tokens,
    value_act,
    gate_act,
    cotangent,
    value_weight,
    gate_weight,
    norm_gain,
    norm_bias,
    mix_weight,
    mix_bias,
):
    value_grad, gate_grad, stats = mixer_backward(
        value_act[0], gate_act[0], cotangent[0], norm_gain, norm_bias, mix_weight, mix_bias
    )
    channels = value_grad.shape[1]
    both_grads = jnp.concatenate((value_grad, gate_grad), axis=1)
    both_weights = jnp.concatenate((value_weight, gate_weight), axis=1)
    input_grad = lax.dot_general(
        both_grads,
        lax.all_gather(both_weights, "dp", axis=0, tiled=True),
        (((1,), (1,)), ((), ())),
        preferred_element_type=jnp.float32,
    ).astype(jnp.bfloat16)
    inputs = tokens[0]
    shard_terms = lax.psum_scatter(
        lax.dot_general(
            inputs, both_grads, (((0,), (0,)), ((), ())), preferred_element_type=jnp.float32
        ),
        "dp",
        scatter_dimension=0,
        tiled=True,
    )
    weight_sums = lax.psum(shard_terms, "sp")
    totals = lax.psum((stats[0], stats[1], stats[2], stats[3]), ("sp", "dp"))
    return (
        input_grad[None],
        weight_sums[:, :channels],
        weight_sums[:, channels:],
        totals[0],
        totals[1],
        totals[2],
        totals[3],
    )


def solution(mesh):
    placed = (
        P("dp", "sp", None),
        P("dp", "sp", None),
        P("dp", "sp", None),
        P("dp", "sp", None),
        P("dp", None),
        P("dp", None),
        P(),
        P(),
        P(),
        P(),
    )
    return jax.shard_map(
        shards,
        mesh=mesh,
        in_specs=placed,
        out_specs=(P("dp", "sp", None), P("dp", None), P("dp", None), P(), P(), P(), P()),
        check_vma=False,
    )
```

profile of v0, /device:TPU:2, one launch (start us, length us, event | category | flops | bytes accessed | tf_op | source)
XLA Modules:
  0.0 603.1 jit_solution(7592910926025882119)
XLA Ops:
  7.2 0.0 copy-start
  7.2 0.0 reduce-scatter.2.cloned.1.call-start
  7.2 2.4 copy.20
  9.6 4.5 fusion.96
  14.2 0.0 copy-done.1
  14.2 0.0 copy-start.14
  14.2 0.0 copy-start.16
  14.2 1.9 convert_multiply_fusion.1
  16.1 0.0 copy-done.14
  16.1 0.1 mul.187
  16.1 0.0 copy-done.16
  16.1 0.1 add.58
  16.2 2.3 copy.28
  18.5 2.3 copy.19
  20.9 0.2 multiply_reduce_fusion.2
  21.1 3.4 reshape.153
  24.6 3.0 convert_multiply_fusion
  27.6 3.6 mul.200
  31.1 3.6 mul.202
  34.7 3.6 mul.177
  38.3 3.6 mul.179
  41.9 5.6 fusion.93
  47.6 0.0 copy-start.9
  47.6 0.0 copy-done.10
  47.6 0.0 copy-done.11
  47.6 0.0 copy-done.12
  47.6 0.0 copy-start.15
  47.6 4.0 multiply_reduce_fusion
  51.6 0.0 copy-start.5
  51.7 1.1 copy-done.5
  52.8 0.5 bitcast_add_fusion
  53.4 1.1 copy.27
  54.5 0.0 copy-done.3
  54.5 0.2 copy-done.4
  54.7 0.8 fusion.78
  55.5 0.0 copy-start.2
  55.5 1.1 copy.36
  56.7 0.3 copy-done.2
  56.9 1.5 fusion.79
  58.5 0.9 copy-done.8
  59.4 0.0 copy-done
  59.4 9.4 %convolution_bitcast_fusion = f32[2048,2048]{0,1:T(8,128)} fusion(bf16[1,384,2048]{2,1,0:T(8,128)(2,1)S(1)} %copy-done, bf16[384,1024]{0,1:T(8,128)(2,1)S(1)} %fusion.79, bf16[384,1024]{0,1:T(8,128)(2,1)S(1)} %fusion.78), kind=kOutput, calls=%fused_computation | convolution fusion | flops 3224371200 | bytes 19922944 | tf_op jit(solution)/shard_map/dot_general | solution.py:88
  68.7 0.0 reduce-scatter.2.cloned.1.call-update
  68.8 0.0 copy-start.6
  68.8 0.0 all-gather.2.cloned.1.call-start
  68.8 0.9 copy-done.13
  69.7 1.8 pad_maximum_fusion.3
  71.5 0.0 all-gather.2.cloned.1.call-update
  71.5 0.0 all-reduce.4.cloned.1.call-start
  71.5 100.9 %reduce-scatter.2.cloned.1.call-done = f32[128,2048]{0,1:T(8,128)} async-done(((f32[2048,2048]{0,1:T(8,128)}), f32[128,2048]{0,1:T(8,128)}) %reduce-scatter.2.cloned.1.call-update) | async-done | bytes 1048592 | tf_op jit(solution)/shard_map/reduce_scatter | solution.py:87
  172.4 0.0 all-reduce.4.cloned.1.call-update
  172.4 0.3 all-reduce.6.cloned.1.call-start
  172.7 2.9 fusion.80
  175.6 0.0 all-reduce.6.cloned.1.call-update
  175.6 0.1 reduce_sum.73
  175.7 0.1 reduce_sum.75
  175.8 77.8 %all-reduce = (f32[16,128]{1,0:T(8,128)}, f32[1024]{0:T(1024)}, f32[1024]{0:T(1024)}) all-reduce(f32[16,128]{1,0:T(8,128)S(1)} %bitcast.235, f32[1024]{0:T(1024)S(1)} %reduce_sum.73, f32[1024]{0:T(1024)S(1)} %reduce_sum.75), channel_id=1, replica_groups=mesh['sp'=16,'dp'=16] {'sp','dp'}, use_global_device_ids=true, to_apply=%region_8.9 | all-reduce | flops 4096 | bytes 32768 | tf_op jit(solution)/shard_map/psum | solution.py:96
  253.6 8.6 %fusion = bf16[1,384,2048]{2,1,0:T(8,128)(2,1)} fusion(bf16[2048,2048]{1,0:T(8,128)(2,1)} %all-gather.2.cloned.1.call-done, bf16[384,1024]{0,1:T(8,128)(2,1)} %copy-done.8, bf16[384,1024]{0,1:T(8,128)(2,1)} %copy-done.7), kind=kOutput, calls=%fused_computation.2 | convolution fusion | flops 3225157632 | bytes 11534336 | tf_op jit(solution)/shard_map/dot_general | solution.py:80
  262.2 67.5 %all-reduce.4.cloned.1.call-done = f32[128,2048]{0,1:T(8,128)} async-done(((f32[128,2048]{0,1:T(8,128)}), f32[128,2048]{0,1:T(8,128)}) %all-reduce.4.cloned.1.call-update) | async-done | bytes 1048592 | tf_op jit(solution)/shard_map/psum | solution.py:95
  329.6 1.3 fusion.98
  330.9 1.0 copy.38
  331.9 1.0 copy.37
  332.9 261.4 %all-reduce.6.cloned.1.call-done = f32[16,128,128]{2,1,0:T(8,128)} async-done(((f32[16,128,128]{2,1,0:T(8,128)}), f32[16,128,128]{2,1,0:T(8,128)}) %all-reduce.6.cloned.1.call-update) | async-done | bytes 1048592 | tf_op jit(solution)/shard_map/psum | solution.py:96
  594.3 2.3 copy.61
  (18 shorter events, 0.1 us)
Async XLA Ops:
  7.2 52.2 %copy-start = (bf16[1,384,2048]{2,1,0:T(8,128)(2,1)S(1)}, bf16[1,384,2048]{2,1,0:T(8,128)(2,1)}, u32[]{:S(2)}) copy-start(bf16[1,384,2048]{2,1,0:T(8,128)(2,1)} %param.10) | copy-start | bytes 4718596
  7.2 165.2 %reduce-scatter.2.cloned.1.call-start = ((), (), s32[]{:S(2)}) async-start(), calls=%async_computation.2 | async-start | bytes 17825792 | tf_op jit(solution)/shard_map/reduce_scatter | solution.py:87
  9.6 4.5 copy-start.1
  14.2 1.9 copy-start.14
  14.2 2.0 copy-start.16
  41.9 5.6 copy-start.10
  41.9 5.6 copy-start.11
  41.9 5.7 copy-start.12
  47.6 4.1 copy-start.9
  47.6 5.2 copy-start.15
  51.6 1.1 copy-start.5
  53.3 1.1 copy-start.3
  53.3 1.4 copy-start.4
  55.5 2.9 copy-start.7
  55.5 1.4 copy-start.2
  58.4 0.9 copy-start.8
  68.7 0.9 copy-start.13
  68.8 103.9 %copy-start.6 = (f32[3,128,16,64]{1,3,0,2:T(8,128)S(1)}, f32[3,128,16,64]{1,3,0,2:T(8,128)}, u32[]{:S(2)}) copy-start(f32[3,128,16,64]{1,3,0,2:T(8,128)} %copy-done.5) | copy-start | bytes 4718596
  68.8 184.8 %all-gather.2.cloned.1.call-start = ((), (), s32[]{:S(2)}) async-start(), calls=%async_computation.1 | async-start | bytes 8912896 | tf_op jit(solution)/shard_map/all_gather | solution.py:82
  71.5 258.2 %all-reduce.4.cloned.1.call-start = ((), (), s32[]{:S(2)}) async-start(), calls=%async_computation.3 | async-start | bytes 2097152 | tf_op jit(solution)/shard_map/psum | solution.py:95
  172.4 421.8 %all-reduce.6.cloned.1.call-start = ((), (), s32[]{:S(2)}) async-start(), calls=%async_computation.4 | async-start | bytes 2097152 | tf_op jit(solution)/shard_map/psum | solution.py:96
Sparse Core Ops, SparseCore 0:
  68.9 103.4 reduce-scatter.1
  174.8 55.9 all-gather.1
  234.0 95.5 all-reduce.3
  335.5 258.7 all-reduce.5
where the time goes:
time: 604 us; the launch traced here: 603 us
  waiting for transfers between devices  430 us (71%)
  blocking collectives  77.8 us (13%)
  local copies, waits for them, and re-layouts  36.4 us (6%)
  matrix products  25.4 us (4%)
  other arithmetic  19.3 us (3%)
  between operations  14 us (2%)
    psum x1, waiting for transfers between devices, shards(): totals = lax.psum((stats[0], stats[1], stats[2], stats[3]), ('sp', 'dp'))  261 us
    reduce_scatter x1, waiting for transfers between devices, shards(): lax.psum_scatter(lax.dot_general(inputs, both_grads, (((0,), (0,)), ((),...  101 us
    psum x1, blocking collectives, shards(): totals = lax.psum((stats[0], stats[1], stats[2], stats[3]), ('sp', 'dp'))  77.8 us
    psum x1, waiting for transfers between devices, shards(): weight_sums = lax.psum(shard_terms, 'sp')  67.5 us
    unnamed x40, local copies, waits for them, and re-layouts  14.9 us
  transfers between devices with their start and end apart: 4, of which 3 were waited for; matrix products, arithmetic and copies ran while one was open for 3% of the time, Pallas kernels for 0%

commit v1 on v0

--- a/solution.py
+++ b/solution.py
@@ -93,7 +93,7 @@
         tiled=True,
     )
     weight_sums = lax.psum(shard_terms, "sp")
-    totals = lax.psum((stats[0], stats[1], stats[2], stats[3]), ("sp", "dp"))
+    totals = lax.psum(lax.psum((stats[0], stats[1], stats[2], stats[3]), "sp"), "dp")
     return (
         input_grad[None],
         weight_sums[:, :channels],

time: 604 us -> 458 us (0.76)
  waiting for transfers between devices: 430 us -> 248 us
  blocking collectives: 77.8 us -> 116 us
    psum x1, waiting for transfers between devices: 261 us -> 103 us  [shards(): lax.psum(lax.psum((stats[0], stats[1], stats[2], stats[3]), 'sp'), 'dp')]
    psum x1, waiting for transfers between devices: 67.5 us -> 0.01 us  [shards(): weight_sums = lax.psum(shard_terms, 'sp')]
    all_gather x1, waiting for transfers between devices: 0.01 us -> 45 us  [shards(): lax.all_gather(both_weights, 'dp', axis=0, tiled=True)]
    psum x1 -> x2, blocking collectives: 77.8 us -> 116 us  [the longest x1 69.5 us: shards(): lax.psum((stats[0], stats[1], stats[2], stats[3]), 'sp')]
    unnamed x40 -> x52, local copies, waits for them, and re-layouts: 14.9 us -> 15.6 us
where the time goes in v1:
time: 458 us; the launch traced here: 456 us
  waiting for transfers between devices  248 us (54%)
  blocking collectives  116 us (25%)
  local copies, waits for them, and re-layouts  36 us (8%)
  matrix products  23.7 us (5%)
  other arithmetic  18.4 us (4%)
  between operations  14 us (3%)
    psum x1, waiting for transfers between devices, shards(): lax.psum(lax.psum((stats[0], stats[1], stats[2], stats[3]), 'sp'), 'dp')  103 us
    reduce_scatter x1, waiting for transfers between devices, shards(): lax.psum_scatter(lax.dot_general(inputs, both_grads, (((0,), (0,)), ((),...  100 us
    psum x1, blocking collectives, shards(): lax.psum((stats[0], stats[1], stats[2], stats[3]), 'sp')  69.5 us
    psum x1, blocking collectives, shards(): lax.psum(lax.psum((stats[0], stats[1], stats[2], stats[3]), 'sp'), 'dp')  46.2 us
    all_gather x1, waiting for transfers between devices, shards(): lax.all_gather(both_weights, 'dp', axis=0, tiled=True)  45 us
    unnamed x52, local copies, waits for them, and re-layouts  15.6 us
    dot_general x1, matrix products, shards(): lax.dot_general(inputs, both_grads, (((0,), (0,)), ((), ())), preferred_e...  9.37 us
  transfers between devices with their start and end apart: 4, of which 3 were waited for; matrix products, arithmetic and copies ran while one was open for 3% of the time, Pallas kernels for 0%

profile of v1, /device:TPU:2, one launch (start us, length us, event | category | flops | bytes accessed | tf_op | source)
XLA Modules:
  0.0 456.4 jit_solution(14912585025921948953)
XLA Ops:
  7.2 0.0 copy-start
  7.2 0.0 reduce-scatter.2.cloned.1.call-start
  7.3 2.4 copy.20
  9.6 4.5 fusion.96
  14.2 0.0 copy-done.2
  14.2 0.0 copy-start.20
  14.2 0.0 copy-start.22
  14.2 1.9 convert_multiply_fusion.1
  16.1 0.1 mul.187
  16.2 0.1 add.66
  16.2 2.3 copy.28
  18.5 2.4 copy.19
  20.9 0.2 multiply_reduce_fusion.2
  21.2 3.5 reshape.153
  24.6 3.0 convert_multiply_fusion
  27.6 3.6 mul.200
  31.2 3.6 mul.202
  34.8 3.6 mul.177
  38.4 3.6 mul.179
  42.0 5.6 %fusion.93 = (f32[128,16]{0,1:T(8,128)S(1)}, bf16[3,128,16,64]{1,3,0,2:T(8,128)(2,1)S(1)}) fusion(f32[3,128,16,64]{1,0,3,2:T(4,128)} %mul.202, f32[3,128,16,64]{1,0,3,2:T(4,128)} %mul.200, f32[3,128,16,64]{1,0,3,2:T(4,128)} %reshape.153), kind=kLoop, calls=%fused_computation.137 | loop fusion | flops 25163776 | bytes 5513216 | tf_op jit(solution)/shard_map/reduce_sum | solution.py:39
  47.7 0.0 copy-start.21
  47.7 4.0 multiply_reduce_fusion
  51.7 0.0 copy-start.6
  51.7 1.1 copy-done.6
  52.9 0.5 bitcast_add_fusion
  53.4 0.0 copy-start.4
  53.4 0.0 copy-start.5
  53.4 1.1 copy.27
  54.5 0.0 copy-done.4
  54.5 0.2 copy-done.5
  54.8 0.8 fusion.78
  55.6 0.0 copy-start.3
  55.6 1.1 copy.36
  56.7 0.3 copy-done.3
  57.0 1.5 fusion.79
  58.5 0.0 copy-done.8
  58.5 0.0 copy-start.10
  58.5 0.9 copy-done.10
  59.4 0.0 copy-done
  59.4 9.4 %convolution_bitcast_fusion = f32[2048,2048]{0,1:T(8,128)} fusion(bf16[1,384,2048]{2,1,0:T(8,128)(2,1)S(1)} %copy-done, bf16[384,1024]{0,1:T(8,128)(2,1)S(1)} %fusion.79, bf16[384,1024]{0,1:T(8,128)(2,1)S(1)} %fusion.78), kind=kOutput, calls=%fused_computation | convolution fusion | flops 3224371200 | bytes 19922944 | tf_op jit(solution)/shard_map/dot_general | solution.py:88
  68.8 0.0 reduce-scatter.2.cloned.1.call-update
  68.8 0.0 all-reduce.8.cloned.1.call-start
  68.9 1.3 copy-done.7
  70.2 0.2 copy-done.13
  70.4 1.8 fusion.80
  72.2 100.3 %reduce-scatter.2.cloned.1.call-done = f32[128,2048]{0,1:T(8,128)} async-done(((f32[2048,2048]{0,1:T(8,128)}), f32[128,2048]{0,1:T(8,128)}) %reduce-scatter.2.cloned.1.call-update) | async-done | bytes 1048592 | tf_op jit(solution)/shard_map/reduce_scatter | solution.py:87
  172.5 0.0 all-reduce.8.cloned.1.call-update
  172.5 0.3 all-gather.2.cloned.1.call-start
  172.8 0.0 copy-done.18
  172.8 0.8 pad_maximum_fusion.3
  173.6 0.0 all-gather.2.cloned.1.call-update
  173.7 0.0 all-reduce.6.cloned.1.call-start
  173.7 0.1 reduce_sum.73
  173.8 0.1 reduce_sum.75
  173.9 69.5 %all-reduce.1 = (f32[16,128]{1,0:T(8,128)S(1)}, f32[1024]{0:T(1024)S(1)}, f32[1024]{0:T(1024)S(1)}) all-reduce(f32[16,128]{1,0:T(8,128)S(1)} %bitcast.235, f32[1024]{0:T(1024)S(1)} %reduce_sum.73, f32[1024]{0:T(1024)S(1)} %reduce_sum.75), channel_id=1, replica_groups=mesh['sp'=16,'dp'=16] {'sp'}, use_global_device_ids=true, to_apply=%region_9.10 | all-reduce | flops 4096 | bytes 32768 | tf_op jit(solution)/shard_map/psum | solution.py:96
  243.3 46.2 %all-reduce = (f32[16,128]{1,0:T(8,128)}, f32[1024]{0:T(1024)}, f32[1024]{0:T(1024)}) all-reduce(f32[16,128]{1,0:T(8,128)S(1)} %get-tuple-element.28, f32[1024]{0:T(1024)S(1)} %get-tuple-element.29, f32[1024]{0:T(1024)S(1)} %get-tuple-element.30), channel_id=1, replica_groups=mesh['sp'=16,'dp'=16] {'dp'}, use_global_device_ids=true, to_apply=%region_10.11 | all-reduce | flops 4096 | bytes 32768 | tf_op jit(solution)/shard_map/psum | solution.py:96
  289.5 0.0 all-reduce.6.cloned.1.call-update
  289.6 45.0 %all-gather.2.cloned.1.call-done = bf16[2048,2048]{1,0:T(8,128)(2,1)} async-done(((bf16[128,2048]{1,0:T(8,128)(2,1)}), bf16[2048,2048]{1,0:T(8,128)(2,1)}) %all-gather.2.cloned.1.call-update) | async-done | bytes 8388624 | tf_op jit(solution)/shard_map/all_gather | solution.py:82
  334.5 8.0 %fusion = bf16[1,384,2048]{2,1,0:T(8,128)(2,1)} fusion(bf16[2048,2048]{1,0:T(8,128)(2,1)} %all-gather.2.cloned.1.call-done, bf16[384,1024]{0,1:T(8,128)(2,1)S(1)} %copy-done.11, bf16[384,1024]{0,1:T(8,128)(2,1)S(1)} %copy-done.9), kind=kOutput, calls=%fused_computation.2 | convolution fusion | flops 3225157632 | bytes 11534336 | tf_op jit(solution)/shard_map/dot_general | solution.py:80
  342.5 0.1 fusion.98
  342.6 1.0 copy.38
  343.6 1.0 copy.37
  344.6 102.9 %all-reduce.6.cloned.1.call-done = f32[16,128,128]{2,1,0:T(8,128)} async-done(((f32[16,128,128]{2,1,0:T(8,128)}), f32[16,128,128]{2,1,0:T(8,128)}) %all-reduce.6.cloned.1.call-update) | async-done | bytes 1048592 | tf_op jit(solution)/shard_map/psum | solution.py:96
  447.5 2.3 copy.62
  (31 shorter events, 0.1 us)
Async XLA Ops:
  7.2 52.3 %copy-start = (bf16[1,384,2048]{2,1,0:T(8,128)(2,1)S(1)}, bf16[1,384,2048]{2,1,0:T(8,128)(2,1)}, u32[]{:S(2)}) copy-start(bf16[1,384,2048]{2,1,0:T(8,128)(2,1)} %param.10) | copy-start | bytes 4718596
  7.2 165.3 %reduce-scatter.2.cloned.1.call-start = ((), (), s32[]{:S(2)}) async-start(), calls=%async_computation.2 | async-start | bytes 17825792 | tf_op jit(solution)/shard_map/reduce_scatter | solution.py:87
  9.6 4.5 copy-start.2
  14.2 1.9 copy-start.20
  14.2 2.0 copy-start.22
  42.0 5.6 %copy-start.14 = (f32[3,128,16,64]{1,0,3,2:T(4,128)S(1)}, f32[3,128,16,64]{1,0,3,2:T(4,128)}, u32[]{:S(2)}) copy-start(f32[3,128,16,64]{1,0,3,2:T(4,128)} %mul.177) | copy-start | bytes 4718596
  42.0 5.6 %copy-start.15 = (f32[3,128,16,64]{1,0,3,2:T(4,128)S(1)}, f32[3,128,16,64]{1,0,3,2:T(4,128)}, u32[]{:S(2)}) copy-start(f32[3,128,16,64]{1,0,3,2:T(4,128)} %mul.179) | copy-start | bytes 4718596
  42.0 5.7 %copy-start.17 = (bf16[16,128,128]{2,1,0:T(8,128)(2,1)S(1)}, bf16[16,128,128]{2,1,0:T(8,128)(2,1)}, u32[]{:S(2)}) copy-start(bf16[16,128,128]{2,1,0:T(8,128)(2,1)} %param.18) | copy-start | bytes 1572868
  47.6 4.1 copy-start.12
  47.7 5.2 %copy-start.21 = (f32[16,128]{1,0:T(8,128)S(1)}, f32[16,128]{1,0:T(8,128)}, u32[]{:S(2)}) copy-start(f32[16,128]{1,0:T(8,128)} %param.19) | copy-start | bytes 24580
  51.7 1.1 copy-start.6
  53.4 1.1 copy-start.4
  53.4 1.4 copy-start.5
  55.6 2.9 copy-start.8
  55.6 1.4 copy-start.3
  58.5 0.9 copy-start.10
  68.8 1.4 copy-start.7
  68.8 1.6 copy-start.13
  68.8 220.7 %all-reduce.8.cloned.1.call-start = ((), (), s32[]{:S(2)}) async-start(), calls=%async_computation.4 | async-start | bytes 4194304 | tf_op jit(solution)/shard_map/psum | solution.py:95
  72.2 100.6 %copy-start.18 = (bf16[128,1024]{1,0:T(8,128)(2,1)S(1)}, bf16[128,1024]{1,0:T(8,128)(2,1)}, u32[]{:S(2)}) copy-start(bf16[128,1024]{1,0:T(8,128)(2,1)} %param.15) | copy-start | bytes 786436
  72.2 100.6 %copy-start.19 = (bf16[128,1024]{1,0:T(8,128)(2,1)S(1)}, bf16[128,1024]{1,0:T(8,128)(2,1)}, u32[]{:S(2)}) copy-start(bf16[128,1024]{1,0:T(8,128)(2,1)} %param.14) | copy-start | bytes 786436
  172.5 162.0 %copy-start.9 = (bf16[384,1024]{0,1:T(8,128)(2,1)S(1)}, bf16[384,1024]{0,1:T(8,128)(2,1)}, u32[]{:S(2)}) copy-start(bf16[384,1024]{0,1:T(8,128)(2,1)} %copy-done.8) | copy-start | bytes 2359300
  172.5 162.0 %copy-start.11 = (bf16[384,1024]{0,1:T(8,128)(2,1)S(1)}, bf16[384,1024]{0,1:T(8,128)(2,1)}, u32[]{:S(2)}) copy-start(bf16[384,1024]{0,1:T(8,128)(2,1)} %copy-done.10) | copy-start | bytes 2359300
  172.5 162.0 %all-gather.2.cloned.1.call-start = ((), (), s32[]{:S(2)}) async-start(), calls=%async_computation.1 | async-start | bytes 8912896 | tf_op jit(solution)/shard_map/all_gather | solution.py:82
  173.7 273.9 %all-reduce.6.cloned.1.call-start = ((), (), s32[]{:S(2)}) async-start(), calls=%async_computation.3 | async-start | bytes 2097152 | tf_op jit(solution)/shard_map/psum | solution.py:96
  289.6 53.0 %copy-start.16 = (f32[128,2048]{0,1:T(8,128)S(1)}, f32[128,2048]{0,1:T(8,128)}, u32[]{:S(2)}) copy-start(f32[128,2048]{0,1:T(8,128)} %get-tuple-element.31) | copy-start | bytes 3145732
  343.6 106.2 %copy-start.1 = (bf16[1,384,2048]{2,1,0:T(8,128)(2,1)S(1)}, bf16[1,384,2048]{2,1,0:T(8,128)(2,1)}, u32[]{:S(2)}) copy-start(bf16[1,384,2048]{2,1,0:T(8,128)(2,1)} %param.10) | copy-start | bytes 4718596
Sparse Core Ops, SparseCore 0:
  68.9 103.4 reduce-scatter.1
  176.4 99.9 all-reduce.7
  278.8 55.6 all-gather.1
  336.7 110.7 all-reduce.5
